TPU v7x, 32 devices: a whole 2x2x4 slice. The times are simulated.
32 devices in a mesh: sp: 8 (over z, x), tp: 4 (over y, core).
Axes of the slice: x: 2, y: 2, z: 4, core: 2. Of those that a mesh axis runs over, the one named last changes fastest.
Arguments:
- residual: bfloat16 [2048, 2048], P(('sp', 'tp')), may hold values from -6 to 6
- queries: bfloat16 [2048, 1024], P('sp', 'tp'), may hold values from -8 to 8
- key_pairs: bfloat16 [2048, 512], P('sp', 'tp'), may hold values from -8 to 8
- values: bfloat16 [2048, 512], P('sp', 'tp'), may hold values from -6 to 6
- lambdas: float32 [8], P('tp'), may hold values from 0.3 to 0.8
- head_gain: float32 [128], replicated, may hold values from 0.1 to 1.9
- out_weight: bfloat16 [1024, 2048], replicated, may hold values from -0.1875 to 0.1875
- mixer_gain: float32 [2048], replicated, may hold values from 0.1 to 1.9
- before_gain: float32 [2048], replicated, may hold values from 0.1 to 1.9
- after_gain: float32 [2048], replicated, may hold values from 0.1 to 1.9
- gate_weight: bfloat16 [2048, 5632], P('sp', 'tp'), may hold values from -0.125 to 0.125
- up_weight: bfloat16 [2048, 5632], P('sp', 'tp'), may hold values from -0.125 to 0.125
- down_weight: bfloat16 [5632, 2048], P('tp', 'sp'), may hold values from -0.078125 to 0.078125
Outputs:
- updated: bfloat16 [2048, 2048], P(('sp', 'tp'))
All inputs are finite; a program needn't handle non-finite values.
Results may differ from a plain program's by a relative error of at most 0.014.
Values may be sent and summed in bfloat16 or wider, within the bound.
A program may use at most 128 MiB of HBM per device.

v0:
```python
import math
import jax
import jax.numpy as jnp
from jax import lax
from jax.sharding import PartitionSpec as P

HEAD_DIM = 64


def row_norm(values_in, gain, epsilon):
    mean_square = jnp.mean(values_in * values_in, axis=-1, keepdims=True)
    return values_in * lax.rsqrt(mean_square + epsilon) * gain


def on_device(
    residual,
    queries,
    key_pairs,
    values,
    lambdas,
    head_gain,
    out_weight,
    mixer_gain,
    before_gain,
    after_gain,
    gate_weight,
    up_weight,
    down_weight,
):
    tokens_here = queries.shape[0]
    quarter = residual.shape[0]
    width = 2 * HEAD_DIM
    local_heads = queries.shape[1] // width
    scale = 1.0 / math.sqrt(HEAD_DIM)
    height = local_heads * tokens_here
    query_rows = jnp.transpose(
        queries.reshape(tokens_here, local_heads, 2, HEAD_DIM), (2, 1, 0, 3)
    ).reshape(2, height, HEAD_DIM)
    empty = (
        jnp.full((height,), -1e30, jnp.float32),
        jnp.zeros((height,), jnp.float32),
        jnp.zeros((height, width), jnp.float32),
    )
    state = (empty, empty)
    key_piece = lax.all_gather(key_pairs, "sp", axis=0, tiled=True)
    value_piece = lax.all_gather(values, "sp", axis=0, tiled=True)
    length = key_piece.shape[0]
    span = length
    for split_count in range(1, length + 1):
        if length % split_count == 0 and length // split_count <= 2048:
            span = length // split_count
            break
    key_blocks = key_piece.reshape(length // span, span, 2, HEAD_DIM)
    value_blocks = value_piece.reshape(length // span, span, width)

    def advance(carry, blocks_in):
        key_block, value_block = blocks_in
        renewed = []
        for which in range(2):
            running_top, running_total, running_numer = carry[which]
            score = (
                jnp.dot(
                    query_rows[which], key_block[:, which].T, preferred_element_type=jnp.float32
                )
                * scale
            )
            new_top = jnp.maximum(running_top, jnp.max(score, axis=1))
            shrink = jnp.exp(running_top - new_top)
            expo = jnp.exp(score - new_top[:, None])
            new_total = running_total * shrink + jnp.sum(expo, axis=1)
            new_numer = running_numer * shrink[:, None] + jnp.dot(
                expo.astype(jnp.bfloat16), value_block, preferred_element_type=jnp.float32
            )
            renewed.append((new_top, new_total, new_numer))
        return (tuple(renewed), None)

    state, _ = lax.scan(advance, state, (key_blocks, value_blocks))
    first_map, second_map = state
    lambda_rows = jnp.repeat(lambdas, tokens_here)[:, None]
    attended = first_map[2] / first_map[1][:, None] - lambda_rows * (
        second_map[2] / second_map[1][:, None]
    )
    normed = row_norm(attended, head_gain, 1e-05).astype(jnp.bfloat16)
    head_out = jnp.transpose(normed.reshape(local_heads, tokens_here, width), (1, 0, 2)).reshape(
        tokens_here, local_heads * width
    )
    grouped = head_out.reshape(lax.axis_size("tp"), quarter, local_heads * width)
    mixed = jnp.dot(
        lax.all_to_all(grouped, "tp", split_axis=0, concat_axis=2, tiled=True)[0],
        out_weight,
        preferred_element_type=jnp.float32,
    ).astype(jnp.bfloat16)[None][0]
    stream = residual.astype(jnp.float32) + row_norm(mixed.astype(jnp.float32), mixer_gain, 1e-06)
    normed_in = row_norm(stream, before_gain, 1e-06).astype(jnp.bfloat16)
    gathered = lax.all_gather(normed_in, "tp", axis=0, tiled=True)
    empty_hidden = jnp.zeros((gathered.shape[0], gate_weight.shape[1]), jnp.float32)
    pieces = (
        lax.all_gather(gate_weight, "sp", axis=0, tiled=True),
        lax.all_gather(up_weight, "sp", axis=0, tiled=True),
    )
    columns = lax.slice_in_dim(gathered, 0, pieces[0].shape[0], axis=1)
    gate_part = jnp.dot(columns, pieces[0], preferred_element_type=jnp.float32)
    up_part = jnp.dot(columns, pieces[1], preferred_element_type=jnp.float32)
    gate = empty_hidden + gate_part
    up = empty_hidden + up_part
    down_whole = lax.all_gather(down_weight, "sp", axis=1, tiled=True)
    hidden = (jax.nn.silu(gate) * up).astype(jnp.bfloat16)
    picked = lax.slice_in_dim(hidden, 0, lax.axis_size("tp") * quarter, axis=0)
    channel = lax.psum_scatter(
        jnp.dot(picked, down_whole, preferred_element_type=jnp.float32).astype(jnp.bfloat16),
        "tp",
        scatter_dimension=0,
        tiled=True,
    )
    updated = stream + 0.5 * row_norm(channel.astype(jnp.float32), after_gain, 1e-06)
    return updated.astype(jnp.bfloat16)


def solution(mesh):
    return jax.shard_map(
        on_device,
        mesh=mesh,
        in_specs=(
            P(("sp", "tp"), None),
            P("sp", "tp"),
            P("sp", "tp"),
            P("sp", "tp"),
            P("tp"),
            P(),
            P(),
            P(),
            P(),
            P(),
            P("sp", "tp"),
            P("sp", "tp"),
            P("tp", "sp"),
        ),
        out_specs=P(("sp", "tp"), None),
        check_vma=False,
    )
```

profile of v0, /device:TPU:0, one launch (start us, length us, event | category | flops | bytes accessed | tf_op | source)
XLA Modules:
  0.0 430.2 jit_solution(3633528644462433819)
XLA Ops:
  6.5 0.0 copy-start
  6.5 0.9 copy.16
  7.5 33.0 %all_gather.18 = bf16[2048,128]{0,1:T(8,128)(2,1)S(1)} all-gather(bf16[256,128]{0,1:T(8,128)(2,1)S(1)} %copy.16), channel_id=1, replica_groups=mesh['sp'=8,'tp'=4] {'sp'}, dimensions={0}, use_global_device_ids=true | all-gather | bytes 589824 | tf_op jit(solution)/shard_map/all_gather | solution.py:45
  40.5 1.0 copy.14
  41.6 0.1 copy.15
  41.7 0.0 copy-start.3
  41.7 0.8 multiply_reduce_fusion.1
  42.5 0.8 fusion
  43.3 31.3 %all_gather.19 = bf16[2048,128]{1,0:T(8,128)(2,1)S(1)} all-gather(bf16[256,128]{1,0:T(8,128)(2,1)S(1)} %copy-done.3), channel_id=1, replica_groups=mesh['sp'=8,'tp'=4] {'sp'}, dimensions={0}, use_global_device_ids=true | all-gather | bytes 589824 | tf_op jit(solution)/shard_map/all_gather | solution.py:46
  74.6 0.1 copy.17
  74.7 0.8 multiply_reduce_fusion
  75.5 0.8 fusion.2
  76.4 0.0 copy-done
  76.4 0.1 broadcast_bitcast_fusion
  76.5 0.9 fusion.29
  77.3 0.0 copy-start.6
  77.4 1.5 multiply_reduce_fusion.4
  78.8 0.0 copy-start.1
  78.9 0.0 copy-start.2
  78.9 0.0 copy-start.4
  78.9 0.1 multiply_convert_fusion.1
  79.0 0.1 copy.25
  79.2 0.1 reshape_reshape.3
  79.3 7.2 %all_to_all.15 = bf16[4,64,256]{2,1,0:T(8,128)(2,1)S(1)} all-to-all(bf16[4,64,256]{2,1,0:T(8,128)(2,1)S(1)} %reshape_reshape.3), channel_id=1, replica_groups=mesh['sp'=8,'tp'=4] {'tp'}, dimensions={0} | all-to-all | bytes 262144 | tf_op jit(solution)/shard_map/all_to_all | solution.py:89
  86.5 0.1 copy.19
  86.6 3.1 multiply_reduce_fusion.3
  89.8 0.0 copy-done.2
  89.8 0.3 multiply_reduce_fusion.2
  90.1 0.9 multiply_convert_fusion
  91.0 0.0 all-gather.5.cloned.1.call-update
  91.0 0.0 all-gather.7.cloned.1.call-start
  91.0 0.7 all-gather.7.cloned.1.call-update
  91.8 0.0 all-gather.11.cloned.1.call-start
  91.8 0.7 all-gather.11.cloned.1.call-update
  92.5 0.0 all-gather.9.cloned.1.call-start
  92.5 0.5 all-gather.9.cloned.1.call-update
  93.1 0.0 reduce-scatter.2.cloned.1.call-start
  93.1 15.0 %all-gather.5.cloned.1.call-done = bf16[256,2048]{1,0:T(8,128)(2,1)} async-done(((bf16[64,2048]{1,0:T(8,128)(2,1)}), bf16[256,2048]{1,0:T(8,128)(2,1)}) %all-gather.5.cloned.1.call-update) | async-done | bytes 1048592 | tf_op jit(solution)/shard_map/all_gather | solution.py:95
  108.1 94.5 %all-gather.7.cloned.1.call-done = bf16[2048,1408]{1,0:T(8,128)(2,1)} async-done(((bf16[256,1408]{1,0:T(8,128)(2,1)}), bf16[2048,1408]{1,0:T(8,128)(2,1)}) %all-gather.7.cloned.1.call-update) | async-done | bytes 5767184 | tf_op jit(solution)/shard_map/all_gather | solution.py:98
  202.6 4.8 %fusion.45 = f32[256,1408]{1,0:T(8,128)S(1)} fusion(bf16[256,2048]{1,0:T(8,128)(2,1)} %all-gather.5.cloned.1.call-done, bf16[2048,1408]{1,0:T(8,128)(2,1)} %all-gather.7.cloned.1.call-done), kind=kOutput, calls=%fused_computation.58 | convolution fusion | flops 1476395008 | bytes 8257536 | tf_op jit(solution)/shard_map/dot_general | solution.py:102
  207.4 0.0 copy-start.5
  207.4 88.6 %all-gather.11.cloned.1.call-done = bf16[1408,2048]{1,0:T(8,128)(2,1)} async-done(((bf16[1408,256]{1,0:T(8,128)(2,1)}), bf16[1408,2048]{1,0:T(8,128)(2,1)}) %all-gather.11.cloned.1.call-update) | async-done | bytes 5767184 | tf_op jit(solution)/shard_map/all_gather | solution.py:106
  296.0 92.6 %all-gather.9.cloned.1.call-done = bf16[2048,1408]{1,0:T(8,128)(2,1)} async-done(((bf16[256,1408]{1,0:T(8,128)(2,1)}), bf16[2048,1408]{1,0:T(8,128)(2,1)}) %all-gather.9.cloned.1.call-update) | async-done | bytes 5767184 | tf_op jit(solution)/shard_map/all_gather | solution.py:99
  388.6 8.9 %convolution_convert_fusion = bf16[256,2048]{1,0:T(8,128)(2,1)} fusion(bf16[1408,2048]{1,0:T(8,128)(2,1)} %all-gather.11.cloned.1.call-done, bf16[256,2048]{1,0:T(8,128)(2,1)S(1)} %copy-done.7, bf16[2048,1408]{1,0:T(8,128)(2,1)} %all-gather.9.cloned.1.call-done, f32[256,1408]{1,0:T(8,128)S(1)} %fusion.45), kind=kOutput, calls=%fused_computation.10 | convolution fusion | flops 2955476992 | bytes 15073280 | tf_op jit(solution)/shard_map/dot_general | solution.py:110
  397.5 0.0 reduce-scatter.2.cloned.1.call-update
  397.5 23.1 %reduce-scatter.2.cloned.1.call-done = bf16[64,2048]{1,0:T(8,128)(2,1)} async-done(((bf16[256,2048]{1,0:T(8,128)(2,1)}), bf16[64,2048]{1,0:T(8,128)(2,1)}) %reduce-scatter.2.cloned.1.call-update) | async-done | bytes 262160 | tf_op jit(solution)/shard_map/reduce_scatter | solution.py:109
  420.6 1.1 fusion.32
  421.7 1.9 fusion.36
  (21 shorter events, 0.1 us)
Async XLA Ops:
  6.5 69.8 %copy-start = (f32[2]{0:T(128)S(1)}, f32[2]{0:T(128)}, u32[]{:S(2)}) copy-start(f32[2]{0:T(128)} %param.17) | copy-start | bytes 28
  6.5 101.6 %all-gather.5.cloned.1.call-start = ((), (), s32[]{:S(2)}) async-start(), calls=%async_computation.2 | async-start | bytes 1310720 | tf_op jit(solution)/shard_map/all_gather | solution.py:95
  41.7 1.7 copy-start.3
  77.3 1.6 copy-start.6
  78.8 10.9 %copy-start.1 = (bf16[64,2048]{1,0:T(8,128)(2,1)S(1)}, bf16[64,2048]{1,0:T(8,128)(2,1)}, u32[]{:S(2)}) copy-start(bf16[64,2048]{1,0:T(8,128)(2,1)} %param.13) | copy-start | bytes 786436
  78.9 10.9 %copy-start.2 = (f32[2048]{0:T(1024)S(1)}, f32[2048]{0:T(1024)}, u32[]{:S(2)}) copy-start(f32[2048]{0:T(1024)} %param.20) | copy-start | bytes 24580
  78.9 11.2 %copy-start.4 = (f32[2048]{0:T(1024)S(1)}, f32[2048]{0:T(1024)}, u32[]{:S(2)}) copy-start(f32[2048]{0:T(1024)} %param.21) | copy-start | bytes 24580
  91.0 111.6 %all-gather.7.cloned.1.call-start = ((), (), s32[]{:S(2)}) async-start(), calls=%async_computation.3 | async-start | bytes 6488064 | tf_op jit(solution)/shard_map/all_gather | solution.py:98
  91.8 204.3 %all-gather.11.cloned.1.call-start = ((), (), s32[]{:S(2)}) async-start(), calls=%async_computation.5 | async-start | bytes 6488064 | tf_op jit(solution)/shard_map/all_gather | solution.py:106
  92.5 296.1 %all-gather.9.cloned.1.call-start = ((), (), s32[]{:S(2)}) async-start(), calls=%async_computation.4 | async-start | bytes 6488064 | tf_op jit(solution)/shard_map/all_gather | solution.py:99
  93.1 327.5 %reduce-scatter.2.cloned.1.call-start = ((), (), s32[]{:S(2)}) async-start(), calls=%async_computation.6 | async-start | bytes 1310720 | tf_op jit(solution)/shard_map/reduce_scatter | solution.py:109
  108.1 280.5 %copy-start.7 = (bf16[256,2048]{1,0:T(8,128)(2,1)S(1)}, bf16[256,2048]{1,0:T(8,128)(2,1)}, u32[]{:S(2)}) copy-start(bf16[256,2048]{1,0:T(8,128)(2,1)} %all-gather.5.cloned.1.call-done) | copy-start | bytes 3145732
  207.4 214.3 %copy-start.5 = (f32[2048]{0:T(1024)S(1)}, f32[2048]{0:T(1024)}, u32[]{:S(2)}) copy-start(f32[2048]{0:T(1024)} %param.22) | copy-start | bytes 24580
Sparse Core Ops, SparseCore 0:
  91.1 16.9 all-gather.4
  110.3 92.2 all-gather.6
  204.7 91.2 all-gather.10
  298.1 90.4 all-gather.8
  397.6 22.9 reduce-scatter.1
where the time goes:
time: 431 us; the launch traced here: 430 us
  waiting for transfers between devices  316 us (73%)
  blocking collectives  71.5 us (17%)
  matrix products  20.8 us (5%)
  between operations  13.4 us (3%)
  other arithmetic  6.02 us (1%)
    all_gather x1, waiting for transfers between devices, on_device(): lax.all_gather(gate_weight, 'sp', axis=0, tiled=True)  94.5 us
    all_gather x1, waiting for transfers between devices, on_device(): lax.all_gather(up_weight, 'sp', axis=0, tiled=True)  92.6 us
    all_gather x1, waiting for transfers between devices, on_device(): down_whole = lax.all_gather(down_weight, 'sp', axis=1, tiled=True)  88.6 us
    all_gather x1, blocking collectives, on_device(): key_piece = lax.all_gather(key_pairs, 'sp', axis=0, tiled=True)  33 us
    all_gather x1, blocking collectives, on_device(): value_piece = lax.all_gather(values, 'sp', axis=0, tiled=True)  31.3 us
    reduce_scatter x1, waiting for transfers between devices, on_device(): lax.psum_scatter(jnp.dot(picked, down_whole, preferred_element_type=jnp.f...  23.1 us
    all_gather x1, waiting for transfers between devices, on_device(): gathered = lax.all_gather(normed_in, 'tp', axis=0, tiled=True)  15 us
    dot_general x1, matrix products, on_device(): jnp.dot(picked, down_whole, preferred_element_type=jnp.float32)  8.9 us
  transfers between devices with their start and end apart: 5, of which 5 were waited for; matrix products, arithmetic and copies ran while one was open for 1% of the time, Pallas kernels for 0%

commit v1 on v0

--- a/solution.py
+++ b/solution.py
@@ -103,7 +103,13 @@
     up_part = jnp.dot(columns, pieces[1], preferred_element_type=jnp.float32)
     gate = empty_hidden + gate_part
     up = empty_hidden + up_part
-    down_whole = lax.all_gather(down_weight, "sp", axis=1, tiled=True)
+    size = lax.axis_size("sp")
+    held, tiles = (down_weight, [down_weight])
+    for _ in range(size - 1):
+        held = lax.ppermute(held, "sp", [(i, (i + 1) % size) for i in range(size)])
+        tiles.insert(0, held)
+    merged = jnp.concatenate(tiles, axis=1)
+    down_whole = jnp.roll(merged, (lax.axis_index("sp") + 1) * down_weight.shape[1], axis=1)
     hidden = (jax.nn.silu(gate) * up).astype(jnp.bfloat16)
     picked = lax.slice_in_dim(hidden, 0, lax.axis_size("tp") * quarter, axis=0)
     channel = lax.psum_scatter(

time: 431 us -> 408 us (0.947)
  waiting for transfers between devices: 316 us -> 265 us
  local copies, waits for them, and re-layouts: 2.59 us -> 26.7 us
    ppermute x0 -> x7, waiting for transfers between devices: none -> 207 us  [on_device(): held = lax.ppermute(held, 'sp', [(i, (i + 1) % size) for i in range(size)])]
    all_gather x1, waiting for transfers between devices: 94.5 us -> 0.01 us  [on_device(): lax.all_gather(gate_weight, 'sp', axis=0, tiled=True)]
    all_gather x1 -> x0, waiting for transfers between devices: 88.6 us -> none  [on_device(): down_whole = lax.all_gather(down_weight, 'sp', axis=1, tiled=True)]
    all_gather x1, waiting for transfers between devices: 92.6 us -> 33.9 us  [on_device(): lax.all_gather(up_weight, 'sp', axis=0, tiled=True)]
    unnamed x23 -> x48, local copies, waits for them, and re-layouts: 2.11 us -> 25.2 us
    all_gather x1, waiting for transfers between devices: 15 us -> 0.01 us  [on_device(): gathered = lax.all_gather(normed_in, 'tp', axis=0, tiled=True)]
  transfers between devices with their start and end apart: 5 -> 11, of which waited for: 5 -> 9; matrix products, arithmetic and copies ran while one was open for 1% -> 7% of each run, Pallas kernels for 0% -> 0%
where the time goes in v1:
time: 408 us; the launch traced here: 407 us
  waiting for transfers between devices  265 us (65%)
  blocking collectives  71.8 us (18%)
  local copies, waits for them, and re-layouts  26.7 us (7%)
  matrix products  22.3 us (5%)
  between operations  13.4 us (3%)
  other arithmetic  6.02 us (1%)
    ppermute x7, waiting for transfers between devices, on_device(): held = lax.ppermute(held, 'sp', [(i, (i + 1) % size) for i in range(size)])  207 us
    all_gather x1, waiting for transfers between devices, on_device(): lax.all_gather(up_weight, 'sp', axis=0, tiled=True)  33.9 us
    all_gather x1, blocking collectives, on_device(): value_piece = lax.all_gather(values, 'sp', axis=0, tiled=True)  33.4 us
    all_gather x1, blocking collectives, on_device(): key_piece = lax.all_gather(key_pairs, 'sp', axis=0, tiled=True)  31.2 us
    unnamed x48, local copies, waits for them, and re-layouts  25.2 us
    reduce_scatter x1, waiting for transfers between devices, on_device(): lax.psum_scatter(jnp.dot(picked, down_whole, preferred_element_type=jnp.f...  23.2 us
    dot_general x1, matrix products, on_device(): jnp.dot(picked, down_whole, preferred_element_type=jnp.float32)  9.22 us
  transfers between devices with their start and end apart: 11, of which 9 were waited for; matrix products, arithmetic and copies ran while one was open for 7% of the time, Pallas kernels for 0%

profile of v1, /device:TPU:0, one launch (start us, length us, event | category | flops | bytes accessed | tf_op | source)
XLA Modules:
  0.0 407.3 jit_solution(9847988821750489172)
XLA Ops:
  6.5 33.4 %all_gather.16 = bf16[2048,128]{1,0:T(8,128)(2,1)S(1)} all-gather(bf16[256,128]{1,0:T(8,128)(2,1)} %param.16), channel_id=1, replica_groups=mesh['sp'=8,'tp'=4] {'sp'}, dimensions={0}, use_global_device_ids=true | all-gather | bytes 589824 | tf_op jit(solution)/shard_map/all_gather | solution.py:46
  39.9 1.0 copy.14
  41.1 0.9 copy.16
  42.0 31.2 %all_gather.15 = bf16[2048,128]{0,1:T(8,128)(2,1)S(1)} all-gather(bf16[256,128]{0,1:T(8,128)(2,1)S(1)} %copy.16), channel_id=1, replica_groups=mesh['sp'=8,'tp'=4] {'sp'}, dimensions={0}, use_global_device_ids=true | all-gather | bytes 589824 | tf_op jit(solution)/shard_map/all_gather | solution.py:45
  73.2 0.8 multiply_reduce_fusion.1
  74.0 0.8 fusion.2
  75.0 0.8 multiply_reduce_fusion
  75.8 0.8 fusion.4
  76.7 0.9 fusion.34
  77.7 1.5 multiply_reduce_fusion.4
  79.6 7.2 %all_to_all.15 = bf16[4,64,256]{2,1,0:T(8,128)(2,1)S(1)} all-to-all(bf16[4,64,256]{2,1,0:T(8,128)(2,1)S(1)} %reshape_reshape.3), channel_id=1, replica_groups=mesh['sp'=8,'tp'=4] {'tp'}, dimensions={0} | all-to-all | bytes 262144 | tf_op jit(solution)/shard_map/all_to_all | solution.py:89
  86.9 3.1 multiply_reduce_fusion.3
  90.1 0.3 multiply_reduce_fusion.2
  90.4 0.9 multiply_convert_fusion
  91.3 0.7 all-gather.6.cloned.1.call-update
  92.1 0.7 all-gather.8.cloned.1.call-update
  92.8 1.9 collective-permute-start
  94.7 18.5 %collective-permute-done = bf16[1408,256]{1,0:T(8,128)(2,1)S(1)} collective-permute-done((bf16[1408,256]{1,0:T(8,128)(2,1)S(1)}, bf16[1408,256]{1,0:T(8,128)(2,1)S(1)}, u32[]{:S(2)}, u32[]{:S(2)}) %collective-permute-start) | collective-permute-done | bytes 720928 | tf_op jit(solution)/shard_map/ppermute | solution.py:109
  113.2 30.2 %collective-permute-done.1 = bf16[1408,256]{1,0:T(8,128)(2,1)S(1)} collective-permute-done((bf16[1408,256]{1,0:T(8,128)(2,1)S(1)}, bf16[1408,256]{1,0:T(8,128)(2,1)S(1)}, u32[]{:S(2)}, u32[]{:S(2)}) %collective-permute-start.1) | collective-permute-done | bytes 720928 | tf_op jit(solution)/shard_map/ppermute | solution.py:109
  143.4 28.0 %collective-permute-done.2 = bf16[1408,256]{1,0:T(8,128)(2,1)S(1)} collective-permute-done((bf16[1408,256]{1,0:T(8,128)(2,1)S(1)}, bf16[1408,256]{1,0:T(8,128)(2,1)S(1)}, u32[]{:S(2)}, u32[]{:S(2)}) %collective-permute-start.2) | collective-permute-done | bytes 720928 | tf_op jit(solution)/shard_map/ppermute | solution.py:109
  171.4 35.6 %collective-permute-done.3 = bf16[1408,256]{1,0:T(8,128)(2,1)S(1)} collective-permute-done((bf16[1408,256]{1,0:T(8,128)(2,1)S(1)}, bf16[1408,256]{1,0:T(8,128)(2,1)S(1)}, u32[]{:S(2)}, u32[]{:S(2)}) %collective-permute-start.3) | collective-permute-done | bytes 720928 | tf_op jit(solution)/shard_map/ppermute | solution.py:109
  207.0 0.9 copy-done.2
  207.9 35.3 %collective-permute-done.4 = bf16[1408,256]{1,0:T(8,128)(2,1)S(1)} collective-permute-done((bf16[1408,256]{1,0:T(8,128)(2,1)S(1)}, bf16[1408,256]{1,0:T(8,128)(2,1)S(1)}, u32[]{:S(2)}, u32[]{:S(2)}) %collective-permute-start.4) | collective-permute-done | bytes 720928 | tf_op jit(solution)/shard_map/ppermute | solution.py:109
  243.2 0.9 copy-done.4
  244.0 23.2 %collective-permute-done.5 = bf16[1408,256]{1,0:T(8,128)(2,1)} collective-permute-done((bf16[1408,256]{1,0:T(8,128)(2,1)S(1)}, bf16[1408,256]{1,0:T(8,128)(2,1)}, u32[]{:S(2)}, u32[]{:S(2)}) %collective-permute-start.5) | collective-permute-done | bytes 720928 | tf_op jit(solution)/shard_map/ppermute | solution.py:109
  267.2 35.9 %collective-permute-done.6 = bf16[1408,256]{1,0:T(8,128)(2,1)} collective-permute-done((bf16[1408,256]{1,0:T(8,128)(2,1)}, bf16[1408,256]{1,0:T(8,128)(2,1)}, u32[]{:S(2)}, u32[]{:S(2)}) %collective-permute-start.6) | collective-permute-done | bytes 720928 | tf_op jit(solution)/shard_map/ppermute | solution.py:109
  303.1 2.1 constant_dynamic-update-slice_fusion.15
  305.2 2.1 constant_dynamic-update-slice_fusion.14
  307.2 2.1 constant_dynamic-update-slice_fusion.13
  309.4 2.2 constant_dynamic-update-slice_fusion.12
  311.5 1.0 constant_dynamic-update-slice_fusion.11
  312.5 1.0 constant_dynamic-update-slice_fusion.10
  313.5 1.0 constant_dynamic-update-slice_fusion.9
  314.4 0.9 constant_dynamic-update-slice_fusion.8
  315.4 2.1 constant_dynamic-update-slice_fusion.7
  317.4 2.1 constant_dynamic-update-slice_fusion.6
  319.5 1.0 constant_dynamic-update-slice_fusion.5
  320.5 1.0 constant_dynamic-update-slice_fusion.4
  321.5 1.0 constant_dynamic-update-slice_fusion.3
  322.5 1.0 constant_dynamic-update-slice_fusion.2
  323.5 1.0 constant_dynamic-update-slice_fusion.1
  324.5 1.0 constant_dynamic-update-slice_fusion
  325.5 5.9 %fusion.51 = f32[256,1408]{1,0:T(8,128)} fusion(bf16[256,2048]{1,0:T(8,128)(2,1)} %all-gather.4.cloned.1.call-done, bf16[2048,1408]{1,0:T(8,128)(2,1)} %all-gather.6.cloned.1.call-done), kind=kOutput, calls=%fused_computation.77 | convolution fusion | flops 1476395008 | bytes 8257536 | tf_op jit(solution)/shard_map/dot_general | solution.py:102
  331.4 33.9 %all-gather.8.cloned.1.call-done = bf16[2048,1408]{1,0:T(8,128)(2,1)} async-done(((bf16[256,1408]{1,0:T(8,128)(2,1)}), bf16[2048,1408]{1,0:T(8,128)(2,1)}) %all-gather.8.cloned.1.call-update) | async-done | bytes 5767184 | tf_op jit(solution)/shard_map/all_gather | solution.py:99
  365.3 9.2 %fusion.7 = bf16[256,2048]{1,0:T(8,128)(2,1)} fusion(bf16[1408,4096]{1,0:T(8,128)(2,1)} %constant_dynamic-update-slice_fusion, s32[]{:T(128)S(6)} %select_n.14, bf16[256,2048]{1,0:T(8,128)(2,1)S(1)} %copy-done.12, bf16[2048,1408]{1,0:T(8,128)(2,1)} %all-gather.8.cloned.1.call-done, f32[256,1408]{1,0:T(8,128)} %fusion.51), kind=kOutput, calls=%fused_computation.12 | convolution fusion | flops 2955476992 | bytes 15073284 | tf_op jit(solution)/shard_map/dot_general | solution.py:116
  374.6 23.2 %reduce-scatter.2.cloned.1.call-done = bf16[64,2048]{1,0:T(8,128)(2,1)} async-done(((bf16[256,2048]{1,0:T(8,128)(2,1)}), bf16[64,2048]{1,0:T(8,128)(2,1)}) %reduce-scatter.2.cloned.1.call-update) | async-done | bytes 262160 | tf_op jit(solution)/shard_map/reduce_scatter | solution.py:115
  397.7 1.1 fusion.37
  398.9 1.9 fusion.41
  (58 shorter events, 1.0 us)
Async XLA Ops:
  6.5 70.1 %copy-start = (f32[2]{0:T(128)S(1)}, f32[2]{0:T(128)}, u32[]{:S(2)}) copy-start(f32[2]{0:T(128)} %param.17) | copy-start | bytes 28
  6.5 318.9 %all-gather.4.cloned.1.call-start = ((), (), s32[]{:S(2)}) async-start(), calls=%async_computation.2 | async-start | bytes 1310720 | tf_op jit(solution)/shard_map/all_gather | solution.py:95
  76.7 2.5 copy-start.11
  77.6 12.4 %copy-start.6 = (bf16[64,2048]{1,0:T(8,128)(2,1)S(1)}, bf16[64,2048]{1,0:T(8,128)(2,1)}, u32[]{:S(2)}) copy-start(bf16[64,2048]{1,0:T(8,128)(2,1)} %param.13) | copy-start | bytes 786436
  77.7 12.4 %copy-start.8 = (f32[2048]{0:T(1024)S(1)}, f32[2048]{0:T(1024)}, u32[]{:S(2)}) copy-start(f32[2048]{0:T(1024)} %param.20) | copy-start | bytes 24580
  77.7 12.7 %copy-start.9 = (f32[2048]{0:T(1024)S(1)}, f32[2048]{0:T(1024)}, u32[]{:S(2)}) copy-start(f32[2048]{0:T(1024)} %param.21) | copy-start | bytes 24580
  79.2 13.6 %copy-start.1 = (bf16[1408,256]{1,0:T(8,128)(2,1)S(1)}, bf16[1408,256]{1,0:T(8,128)(2,1)}, u32[]{:S(2)}) copy-start(bf16[1408,256]{1,0:T(8,128)(2,1)} %param.25) | copy-start | bytes 2162692
  91.3 234.2 %all-gather.6.cloned.1.call-start = ((), (), s32[]{:S(2)}) async-start(), calls=%async_computation.3 | async-start | bytes 6488064 | tf_op jit(solution)/shard_map/all_gather | solution.py:98
  92.0 273.3 %all-gather.8.cloned.1.call-start = ((), (), s32[]{:S(2)}) async-start(), calls=%async_computation.4 | async-start | bytes 6488064 | tf_op jit(solution)/shard_map/all_gather | solution.py:99
  92.8 305.0 %reduce-scatter.2.cloned.1.call-start = ((), (), s32[]{:S(2)}) async-start(), calls=%async_computation.5 | async-start | bytes 1310720 | tf_op jit(solution)/shard_map/reduce_scatter | solution.py:115
  92.8 20.4 %collective-permute-start = (bf16[1408,256]{1,0:T(8,128)(2,1)S(1)}, bf16[1408,256]{1,0:T(8,128)(2,1)S(1)}, u32[]{:S(2)}, u32[]{:S(2)}) collective-permute-start(bf16[1408,256]{1,0:T(8,128)(2,1)S(1)} %copy-done.1), channel_id=1, source_target_pairs={{0,4},{4,8},{8,12},{12,16},{16,20},{20,24},{24,28},{28,0},{1,5},{5... | collective-permute-start | bytes 2162696 | tf_op jit(solution)/shard_map/ppermute | solution.py:109
  113.2 30.2 %collective-permute-start.1 = (bf16[1408,256]{1,0:T(8,128)(2,1)S(1)}, bf16[1408,256]{1,0:T(8,128)(2,1)S(1)}, u32[]{:S(2)}, u32[]{:S(2)}) collective-permute-start(bf16[1408,256]{1,0:T(8,128)(2,1)S(1)} %collective-permute-done), channel_id=1, source_target_pairs={{0,4},{4,8},{8,12},{12,16},{16,20},{20,24},{24,28},{28,0},{1,5},{5... | collective-permute-start | bytes 2162696 | tf_op jit(solution)/shard_map/ppermute | solution.py:109
  143.4 28.0 %collective-permute-start.2 = (bf16[1408,256]{1,0:T(8,128)(2,1)S(1)}, bf16[1408,256]{1,0:T(8,128)(2,1)S(1)}, u32[]{:S(2)}, u32[]{:S(2)}) collective-permute-start(bf16[1408,256]{1,0:T(8,128)(2,1)S(1)} %collective-permute-done.1), channel_id=1, source_target_pairs={{0,4},{4,8},{8,12},{12,16},{16,20},{20,24},{24,28},{28,0},{1,5},{5... | collective-permute-start | bytes 2162696 | tf_op jit(solution)/shard_map/ppermute | solution.py:109
  171.4 35.6 %collective-permute-start.3 = (bf16[1408,256]{1,0:T(8,128)(2,1)S(1)}, bf16[1408,256]{1,0:T(8,128)(2,1)S(1)}, u32[]{:S(2)}, u32[]{:S(2)}) collective-permute-start(bf16[1408,256]{1,0:T(8,128)(2,1)S(1)} %collective-permute-done.2), channel_id=1, source_target_pairs={{0,4},{4,8},{8,12},{12,16},{16,20},{20,24},{24,28},{28,0},{1,5},{5... | collective-permute-start | bytes 2162696 | tf_op jit(solution)/shard_map/ppermute | solution.py:109
  207.0 0.9 copy-start.2
  207.9 35.3 %collective-permute-start.4 = (bf16[1408,256]{1,0:T(8,128)(2,1)S(1)}, bf16[1408,256]{1,0:T(8,128)(2,1)S(1)}, u32[]{:S(2)}, u32[]{:S(2)}) collective-permute-start(bf16[1408,256]{1,0:T(8,128)(2,1)S(1)} %collective-permute-done.3), channel_id=1, source_target_pairs={{0,4},{4,8},{8,12},{12,16},{16,20},{20,24},{24,28},{28,0},{1,5},{5... | collective-permute-start | bytes 2162696 | tf_op jit(solution)/shard_map/ppermute | solution.py:109
  243.2 0.9 copy-start.4
  244.0 23.2 %collective-permute-start.5 = (bf16[1408,256]{1,0:T(8,128)(2,1)S(1)}, bf16[1408,256]{1,0:T(8,128)(2,1)}, u32[]{:S(2)}, u32[]{:S(2)}) collective-permute-start(bf16[1408,256]{1,0:T(8,128)(2,1)S(1)} %collective-permute-done.4), channel_id=1, source_target_pairs={{0,4},{4,8},{8,12},{12,16},{16,20},{20,24},{24,28},{28,0},{1,5},{5... | collective-permute-start | bytes 2162696 | tf_op jit(solution)/shard_map/ppermute | solution.py:109
  267.2 35.9 %collective-permute-start.6 = (bf16[1408,256]{1,0:T(8,128)(2,1)}, bf16[1408,256]{1,0:T(8,128)(2,1)}, u32[]{:S(2)}, u32[]{:S(2)}) collective-permute-start(bf16[1408,256]{1,0:T(8,128)(2,1)} %collective-permute-done.5), channel_id=1, source_target_pairs={{0,4},{4,8},{8,12},{12,16},{16,20},{20,24},{24,28},{28,0},{1,5},{5... | collective-permute-start | bytes 2162696 | tf_op jit(solution)/shard_map/ppermute | solution.py:109
  307.2 12.3 %copy-start.5 = (bf16[1408,256]{1,0:T(8,128)(2,1)S(1)}, bf16[1408,256]{1,0:T(8,128)(2,1)}, u32[]{:S(2)}) copy-start(bf16[1408,256]{1,0:T(8,128)(2,1)} %copy-done.4) | copy-start | bytes 2162692
  309.4 11.2 %copy-start.3 = (bf16[1408,256]{1,0:T(8,128)(2,1)S(1)}, bf16[1408,256]{1,0:T(8,128)(2,1)}, u32[]{:S(2)}) copy-start(bf16[1408,256]{1,0:T(8,128)(2,1)} %copy-done.2) | copy-start | bytes 2162692
  325.5 39.9 %copy-start.12 = (bf16[256,2048]{1,0:T(8,128)(2,1)S(1)}, bf16[256,2048]{1,0:T(8,128)(2,1)}, u32[]{:S(2)}) copy-start(bf16[256,2048]{1,0:T(8,128)(2,1)} %all-gather.4.cloned.1.call-done) | copy-start | bytes 3145732
  331.4 67.4 %copy-start.7 = (bf16[64,2048]{1,0:T(8,128)(2,1)S(1)}, bf16[64,2048]{1,0:T(8,128)(2,1)}, u32[]{:S(2)}) copy-start(bf16[64,2048]{1,0:T(8,128)(2,1)} %param.13) | copy-start | bytes 786436
  331.4 67.5 %copy-start.10 = (f32[2048]{0:T(1024)S(1)}, f32[2048]{0:T(1024)}, u32[]{:S(2)}) copy-start(f32[2048]{0:T(1024)} %param.22) | copy-start | bytes 24580
Sparse Core Ops, SparseCore 0:
  91.4 17.0 all-gather.3
  110.6 133.1 all-gather.5
  246.1 119.2 all-gather.7
  374.7 22.9 reduce-scatter.1
